TPU v7x, 32 devices: a whole 2x2x4 slice. The times are simulated.
32 devices in a mesh: grp: 2 (over y), sp: 4 (over z), tp: 4 (over x, core).
Axes of the slice: x: 2, y: 2, z: 4, core: 2. Of those that a mesh axis runs over, the one named last changes fastest.
Arguments:
- conv_input: bfloat16 [4096, 1024], P(('grp', 'sp'), 'tp'), parts along dimension 0, may hold values from -6 to 6
- pre_gate: bfloat16 [4096, 1024], P(('grp', 'sp'), 'tp'), parts along dimension 0, may hold values from -6 to 6
- post_gate: bfloat16 [4096, 1024], P(('grp', 'sp'), 'tp'), parts along dimension 0, may hold values from -6 to 6
- conv_taps: float32 [3, 1024], replicated, may hold values from -3.5 to 3.5
- out_proj: bfloat16 [1024, 2048], replicated, may hold values from -0.1875 to 0.1875
- residual_in: bfloat16 [4096, 2048], P(('grp', 'sp', 'tp')), parts along dimension 0, may hold values from -6 to 6
- norm_gain: float32 [2048], replicated, may hold values from 0.1 to 1.9
- routes: int32 [4096, 2], P(('grp', 'sp', 'tp')), parts along dimension 0, may hold values from 0 to 7, as said below
- route_weight: float32 [4096, 2], P(('grp', 'sp', 'tp')), parts along dimension 0, may hold values from 0.1 to 1
- w_gate: bfloat16 [8, 2048, 1024], P('sp', None, 'tp'), may hold values from -0.125 to 0.125
- w_up: bfloat16 [8, 2048, 1024], P('sp', None, 'tp'), may hold values from -0.125 to 0.125
- w_down: bfloat16 [8, 1024, 2048], P('sp', 'tp'), may hold values from -0.1875 to 0.1875
Outputs:
- layer_out: bfloat16 [4096, 2048], P(('grp', 'sp', 'tp')), parts along dimension 0
There are 2 independent parts, one for each index of `grp`. A program takes and returns all parts, laid end to end along the dimension named above; an argument that names none is the same for every part. Nothing has to cross between parts.
Inputs may be any that keep to these rules, and one draw needn't show every extreme that they name: `routes`: the two numbers of a row differ and lie in the same group of 2 consecutive experts. In each aligned block of 128 rows every expert is named exactly 32 times.
All inputs are finite; a program needn't handle non-finite values.
Results may differ from a plain program's by a relative error of at most 0.0085.
Values may be sent and summed in bfloat16 or wider, within the bound.
No kernel may reach another device: no remote copies, remote signals or barrier semaphores. Data moves between devices by JAX's collectives and lax.ppermute only.
A program may use at most 64 MiB of HBM per device.

v0:
```python
import jax
import jax.numpy as jnp
from jax import lax
from jax.sharding import PartitionSpec as P

GROUPS = 4
LANES = 128


def shifted(block, axis, distance):
    devices = range(lax.axis_size(axis))
    route = [(i - distance, i) for i in devices if i - distance in devices]
    return lax.ppermute(block, axis, route)


def flipped(block, axis, bit):
    return lax.ppermute(block, axis, [(i, i ^ bit) for i in range(lax.axis_size(axis))])


def mix(conv_input, pre_gate, post_gate, conv_taps):
    channels = conv_input.shape[1]
    taps = lax.dynamic_slice_in_dim(conv_taps, lax.axis_index("tp") * channels, channels, 1)
    edge = jnp.concatenate([conv_input[-2:], pre_gate[-2:]], axis=1)
    prior = shifted(edge, "sp", 1)
    prior_input, prior_gate = (prior[:, :channels], prior[:, channels:])
    gated = jnp.concatenate(
        [
            prior_gate.astype(jnp.float32) * prior_input.astype(jnp.float32),
            pre_gate.astype(jnp.float32) * conv_input.astype(jnp.float32),
        ],
        axis=0,
    )
    conv = gated[2:] * taps[2] + gated[1:-1] * taps[1] + gated[:-2] * taps[0]
    return (post_gate.astype(jnp.float32) * conv).astype(jnp.bfloat16)


def project(mixed, out_proj, residual_in, norm_gain):
    token_rows = lax.all_to_all(mixed, "tp", split_axis=0, concat_axis=1, tiled=True)
    projected = jnp.dot(token_rows, out_proj, preferred_element_type=jnp.float32)
    stream = residual_in.astype(jnp.float32) + projected
    scale = lax.rsqrt(jnp.mean(stream * stream, axis=-1, keepdims=True) + 1e-06)
    normed = (stream * scale * norm_gain).astype(jnp.bfloat16)
    return (stream, normed)


def route_by_group(stream, normed, routes, route_weight, w_gate, w_up, w_down):
    shards = lax.axis_size("tp")
    seq_ranks = lax.axis_size("sp")
    block_rows, width = stream.shape
    local_experts = w_gate.shape[0]
    capacity = block_rows // seq_ranks
    group = routes[:, 0] // local_experts
    order = jnp.arange(block_rows, dtype=jnp.int32)
    earlier = (group[:, None] == group[None, :]) & (order[None, :] < order[:, None])
    slot = group * capacity + jnp.sum(earlier.astype(jnp.int32), axis=1)
    select = (order[:, None] == slot[None, :]).astype(jnp.bfloat16)
    member = routes[:, :, None] % local_experts == jnp.arange(local_experts, dtype=jnp.int32)
    weight = jnp.sum(jnp.where(member, route_weight[:, :, None], 0.0), axis=1)
    high = lax.reduce_precision(weight, 8, 7)
    labels = jnp.concatenate([high, weight - high], axis=1).astype(jnp.bfloat16)
    labels = jnp.pad(labels, ((0, 0), (0, LANES - labels.shape[1])))
    rows = jnp.concatenate([normed, labels], axis=1)
    outgoing = jnp.dot(select, rows, preferred_element_type=jnp.float32).astype(jnp.bfloat16)
    outgoing = outgoing.reshape(seq_ranks, capacity, width + LANES)
    arrived = lax.all_to_all(outgoing, "sp", split_axis=0, concat_axis=0, tiled=True)
    blocks = {0: arrived.reshape(block_rows, width + LANES)}
    bits = [1 << b for b in range(shards.bit_length() - 1)]
    for bit in reversed(bits):
        blocks.update({k | bit: flipped(v, "tp", bit) for k, v in blocks.items()})
    down = w_down.reshape(local_experts * w_down.shape[1], width)
    parts = {}
    for k, block in blocks.items():
        features = block[:, :width]
        marks = block[:, width:].astype(jnp.float32)
        hidden = []
        for expert in range(local_experts):
            gate = jnp.dot(features, w_gate[expert], preferred_element_type=jnp.float32)
            upper = jnp.dot(features, w_up[expert], preferred_element_type=jnp.float32)
            scale = marks[:, expert] + marks[:, local_experts + expert]
            hidden.append((jax.nn.silu(gate) * upper * scale[:, None]).astype(jnp.bfloat16))
        hidden = jnp.concatenate(hidden, axis=1)
        parts[k] = jnp.dot(hidden, down, preferred_element_type=jnp.float32)
    for bit in bits:
        for k in [k for k in parts if k & bit]:
            parts[k ^ bit] += flipped(parts.pop(k).astype(jnp.bfloat16), "tp", bit).astype(
                jnp.float32
            )
    summed = parts[0].astype(jnp.bfloat16).reshape(seq_ranks, capacity, width)
    returned = lax.all_to_all(summed, "sp", split_axis=0, concat_axis=0, tiled=True)
    weighted = lax.dot_general(
        select,
        returned.reshape(block_rows, width),
        (((0,), (0,)), ((), ())),
        preferred_element_type=jnp.float32,
    )
    return (stream + weighted).astype(jnp.bfloat16)


def route_by_expert(stream, normed, routes, route_weight, w_gate, w_up, w_down):
    shards = lax.axis_size("tp")
    seq_ranks = lax.axis_size("sp")
    block_rows, width = stream.shape
    local_experts = w_gate.shape[0]
    experts = local_experts * seq_ranks
    capacity = 2 * block_rows // experts
    flat_routes = routes.reshape(-1)
    position = jnp.arange(flat_routes.shape[0], dtype=jnp.int32)
    earlier = (flat_routes[:, None] == flat_routes[None, :]) & (
        position[None, :] < position[:, None]
    )
    rank = jnp.sum(earlier.astype(jnp.int32), axis=1)
    slot = flat_routes * capacity + rank
    outgoing = (
        jnp.zeros((experts * capacity, width), jnp.bfloat16).at[slot].set(normed[position // 2])
    )
    outgoing = outgoing.reshape(seq_ranks, local_experts, capacity, width)
    spread = lax.all_gather(
        lax.all_to_all(outgoing, "sp", split_axis=0, concat_axis=0, tiled=True)[:, None],
        "tp",
        axis=1,
        tiled=True,
    )
    count = spread.shape[3]
    partials = []
    for expert in range(local_experts):
        rows = spread[:, :, expert].reshape(seq_ranks * shards * count, width)
        gate = jnp.dot(rows, w_gate[expert], preferred_element_type=jnp.float32)
        upper = jnp.dot(rows, w_up[expert], preferred_element_type=jnp.float32)
        hidden = (jax.nn.silu(gate) * upper).astype(jnp.bfloat16)
        part = jnp.dot(hidden, w_down[expert], preferred_element_type=jnp.float32).astype(
            jnp.bfloat16
        )
        partials.append(part.reshape(seq_ranks, shards, count, width))
    stacked = jnp.stack(partials, axis=2)
    summed = lax.psum_scatter(stacked, "tp", scatter_dimension=1, tiled=True).astype(jnp.float32)
    returned = lax.all_to_all(
        summed[:, 0].astype(jnp.bfloat16), "sp", split_axis=0, concat_axis=0, tiled=True
    )
    results = returned.reshape(experts * capacity, width)[slot]
    results = results.reshape(block_rows, 2, width).astype(jnp.float32)
    weighted = jnp.sum(route_weight[:, :, None] * results, axis=1)
    return (stream + weighted).astype(jnp.bfloat16)


def on_device(
    conv_input,
    pre_gate,
    post_gate,
    conv_taps,
    out_proj,
    residual_in,
    norm_gain,
    routes,
    route_weight,
    w_gate,
    w_up,
    w_down,
):
    shards = lax.axis_size("tp")
    mixed = mix(conv_input, pre_gate, post_gate, conv_taps)
    stream, normed = project(mixed, out_proj, residual_in, norm_gain)
    whole_groups = lax.axis_size("sp") == GROUPS and shards & shards - 1 == 0
    route = route_by_group if whole_groups else route_by_expert
    return route(stream, normed, routes, route_weight, w_gate, w_up, w_down)


def solution(mesh):
    return jax.shard_map(
        on_device,
        mesh=mesh,
        in_specs=(
            P(("grp", "sp"), "tp"),
            P(("grp", "sp"), "tp"),
            P(("grp", "sp"), "tp"),
            P(),
            P(),
            P(("grp", "sp", "tp"), None),
            P(),
            P(("grp", "sp", "tp"), None),
            P(("grp", "sp", "tp"), None),
            P("sp", None, "tp"),
            P("sp", None, "tp"),
            P("sp", "tp", None),
        ),
        out_specs=P(("grp", "sp", "tp"), None),
        check_vma=False,
    )
```

profile of v0, /device:TPU:0, one launch (start us, length us, event | category | flops | bytes accessed | tf_op | source)
XLA Modules:
  0.0 97.2 jit_solution(9595113881826151975)
XLA Ops:
  0.0 0.8 slice.127
  0.8 0.7 slice.128
  1.5 5.0 %collective-permute-start = (bf16[2,512]{1,0:T(2,128)(2,1)S(1)}, bf16[2,512]{1,0:T(2,128)(2,1)S(1)}, u32[]{:S(2)}, u32[]{:S(2)}) collective-permute-start(bf16[2,512]{1,0:T(2,128)(2,1)S(1)} %pad_maximum_fusion.1), channel_id=1, source_target_pairs={{0,4},{4,8},{8,12},{1,5},{5,9},{9,13},{2,6},{6,10},{10,14},{3,7},{... | collective-permute-start | bytes 6152 | tf_op jit(solution)/shard_map/ppermute | solution.py:13
  6.5 0.7 fusion.111
  7.2 0.7 and_select_fusion.2
  7.9 0.7 and_select_fusion
  8.6 1.1 %convert_multiply_fusion = f32[512,256]{1,0:T(8,128)S(1)} fusion(bf16[512,256]{1,0:T(8,128)(2,1)} %param.12, bf16[512,256]{1,0:T(8,128)(2,1)} %param.13), kind=kLoop, calls=%fused_computation.78 | loop fusion | flops 393216 | bytes 1048576 | tf_op jit(solution)/shard_map/mul | solution.py:29
  9.7 0.7 fusion.108
  10.6 0.9 fusion.119
  11.6 1.9 %fusion.62 = bf16[512,256]{1,0:T(8,128)(2,1)} fusion(f32[2,256]{1,0:T(2,128)S(1)} %convert_multiply_fusion.1, f32[512,256]{1,0:T(8,128)S(1)} %convert_multiply_fusion, bf16[512,256]{1,0:T(8,128)(2,1)} %param.14, f32[256]{0:T(256)S(1)} %bitcast.96, f32[256]{0:T(256)S(1)} %bitcast.95, f32[256]{0:T(256)S(1)} %bitcast.94), kind=kLoop, calls=%fused_computation.75 | loop fusion | flops 1310720 | bytes 1053696 | tf_op jit(solution)/shard_map/convert_element_type | solution.py:34
  13.5 3.4 %all-to-all-start = ((bf16[4,128,256]{2,1,0:T(8,128)(2,1)}), bf16[4,128,256]{2,1,0:T(8,128)(2,1)S(1)}, u32[]{:S(2)}, u32[]{:S(2)}) async-start(bf16[4,128,256]{2,1,0:T(8,128)(2,1)} %bitcast.3), calls=%async_computation | async-start | bytes 524288 | tf_op jit(solution)/shard_map/all_to_all | solution.py:38
  16.9 5.9 %all-to-all-done = bf16[4,128,256]{2,1,0:T(8,128)(2,1)S(1)} async-done(((bf16[4,128,256]{2,1,0:T(8,128)(2,1)}), bf16[4,128,256]{2,1,0:T(8,128)(2,1)S(1)}, u32[]{:S(2)}, u32[]{:S(2)}) %all-to-all-start) | async-done | bytes 262176 | tf_op jit(solution)/shard_map/all_to_all | solution.py:38
  23.0 3.0 %multiply_reduce_fusion = (f32[128]{0:T(128)S(1)}, f32[128,2048]{1,0:T(8,128)S(1)}) fusion(bf16[128,1024]{0,1:T(8,128)(2,1)S(1)} %bitcast.84, bf16[1024,2048]{1,0:T(8,128)(2,1)} %param.16, bf16[128,2048]{1,0:T(8,128)(2,1)S(1)} %copy-done.1), kind=kOutput, calls=%fused_computation.47 | convolution fusion | flops 537919360 | bytes 6029824 | tf_op jit(solution)/shard_map/dot_general | solution.py:39
  26.2 0.3 convolution_convert_fusion
  26.6 18.7 %all_to_all.29 = bf16[4,32,2176]{2,1,0:T(8,128)(2,1)S(1)} all-to-all(bf16[4,32,2176]{2,1,0:T(8,128)(2,1)S(1)} %bitcast.93), channel_id=1, replica_groups=mesh['grp'=2,'sp'=4,'tp'=4] {'sp'}, dimensions={0} | all-to-all | bytes 1114112 | tf_op jit(solution)/shard_map/all_to_all | solution.py:65
  45.3 0.8 collective-permute-start.3
  46.1 0.3 fusion.19
  46.4 0.2 fusion.104
  46.6 0.3 fusion.34
  47.0 0.3 fusion.4
  47.3 0.8 collective-permute-done.1
  48.2 0.3 fusion.17
  48.6 0.3 fusion.32
  48.9 0.3 multiply_convert_fusion.5
  49.2 0.3 multiply_convert_fusion.6
  49.6 0.4 convolution_convert_fusion.2
  50.0 8.4 %collective-permute-done.3 = bf16[128,2176]{1,0:T(8,128)(2,1)S(1)} collective-permute-done((bf16[128,2176]{1,0:T(8,128)(2,1)S(1)}, bf16[128,2176]{1,0:T(8,128)(2,1)S(1)}, u32[]{:S(2)}, u32[]{:S(2)}) %collective-permute-start.3) | collective-permute-done | bytes 557088 | tf_op jit(solution)/shard_map/ppermute | solution.py:17
  58.6 0.6 collective-permute-start.2
  59.2 0.3 fusion.15
  59.5 0.3 multiply_convert_fusion.3
  59.9 0.5 collective-permute-done.4
  60.6 0.3 fusion.13
  60.9 0.3 fusion.28
  61.3 0.3 multiply_convert_fusion.1
  61.6 0.3 multiply_convert_fusion.2
  61.9 0.4 convolution_convert_fusion.1
  62.4 0.2 collective-permute-start.5
  62.6 0.3 fusion.30
  62.9 0.3 multiply_convert_fusion.4
  63.2 1.1 %collective-permute-done.5 = bf16[128,2048]{1,0:T(8,128)(2,1)S(1)} collective-permute-done((bf16[128,2048]{1,0:T(8,128)(2,1)S(1)}, bf16[128,2048]{1,0:T(8,128)(2,1)S(1)}, u32[]{:S(2)}, u32[]{:S(2)}) %collective-permute-start.5) | collective-permute-done | bytes 524320 | tf_op jit(solution)/shard_map/ppermute | solution.py:17
  64.3 0.4 add_convert_fusion.1
  64.8 1.4 %collective-permute-start.6 = (bf16[128,2048]{1,0:T(8,128)(2,1)S(1)}, bf16[128,2048]{1,0:T(8,128)(2,1)S(1)}, u32[]{:S(2)}, u32[]{:S(2)}) collective-permute-start(bf16[128,2048]{1,0:T(8,128)(2,1)S(1)} %add_convert_fusion.1), channel_id=1, source_target_pairs={{0,2},{1,3},{2,0},{3,1},{4,6},{5,7},{6,4},{7,5},{8,10},{9,11},{10,... | collective-permute-start | bytes 1572872 | tf_op jit(solution)/shard_map/ppermute | solution.py:17
  66.2 0.3 fusion.3
  66.5 0.4 fusion.81
  67.0 11.9 %collective-permute-done.6 = bf16[128,2048]{1,0:T(8,128)(2,1)S(1)} collective-permute-done((bf16[128,2048]{1,0:T(8,128)(2,1)S(1)}, bf16[128,2048]{1,0:T(8,128)(2,1)S(1)}, u32[]{:S(2)}, u32[]{:S(2)}) %collective-permute-start.6) | collective-permute-done | bytes 524320 | tf_op jit(solution)/shard_map/ppermute | solution.py:17
  78.8 0.2 add_convert_fusion
  79.0 17.0 %all_to_all.30 = bf16[4,32,2048]{2,1,0:T(8,128)(2,1)S(1)} all-to-all(bf16[4,32,2048]{2,1,0:T(8,128)(2,1)S(1)} %bitcast.82), channel_id=1, replica_groups=mesh['grp'=2,'sp'=4,'tp'=4] {'sp'}, dimensions={0} | all-to-all | bytes 1048576 | tf_op jit(solution)/shard_map/all_to_all | solution.py:89
  96.1 1.1 %fusion = bf16[128,2048]{1,0:T(8,128)(2,1)} fusion(f32[128,2048]{1,0:T(8,128)S(1)} %get-tuple-element.19, bf16[128,2048]{1,0:T(8,128)(2,1)S(1)} %bitcast.83, s32[128]{0:T(128)S(1)} %multiply_add_fusion), kind=kOutput, calls=%fused_computation.3 | convolution fusion | flops 67649536 | bytes 2097664 | tf_op jit(solution)/shard_map/dot_general | solution.py:90
  (33 shorter events, 1.3 us)
Async XLA Ops:
  0.0 49.6 %copy-start = (bf16[2,256,2048]{2,1,0:T(8,128)(2,1)S(1)}, bf16[2,256,2048]{2,1,0:T(8,128)(2,1)}, u32[]{:S(2)}) copy-start(bf16[2,256,2048]{2,1,0:T(8,128)(2,1)} %param.23) | copy-start | bytes 6291460
  0.0 16.9 %copy-start.3 = (s32[128,2]{0,1:T(2,128)S(1)}, s32[128,2]{0,1:T(2,128)}, u32[]{:S(2)}) copy-start(s32[128,2]{0,1:T(2,128)} %param.19) | copy-start | bytes 3076
  0.0 23.0 %copy-start.1 = (bf16[128,2048]{1,0:T(8,128)(2,1)S(1)}, bf16[128,2048]{1,0:T(8,128)(2,1)}, u32[]{:S(2)}) copy-start(bf16[128,2048]{1,0:T(8,128)(2,1)} %param.17) | copy-start | bytes 1572868
  1.5 10.0 %collective-permute-start = (bf16[2,512]{1,0:T(2,128)(2,1)S(1)}, bf16[2,512]{1,0:T(2,128)(2,1)S(1)}, u32[]{:S(2)}, u32[]{:S(2)}) collective-permute-start(bf16[2,512]{1,0:T(2,128)(2,1)S(1)} %pad_maximum_fusion.1), channel_id=1, source_target_pairs={{0,4},{4,8},{8,12},{1,5},{5,9},{9,13},{2,6},{6,10},{10,14},{3,7},{... | collective-permute-start | bytes 6152 | tf_op jit(solution)/shard_map/ppermute | solution.py:13
  13.5 9.4 %all-to-all-start = ((bf16[4,128,256]{2,1,0:T(8,128)(2,1)}), bf16[4,128,256]{2,1,0:T(8,128)(2,1)S(1)}, u32[]{:S(2)}, u32[]{:S(2)}) async-start(bf16[4,128,256]{2,1,0:T(8,128)(2,1)} %bitcast.3), calls=%async_computation | async-start | bytes 524288 | tf_op jit(solution)/shard_map/all_to_all | solution.py:38
  23.0 3.0 %copy-start.2 = (f32[2048]{0:T(1024)S(1)}, f32[2048]{0:T(1024)}, u32[]{:S(2)}) copy-start(f32[2048]{0:T(1024)} %param.18) | copy-start | bytes 24580
  26.1 20.0 %copy-start.4 = (bf16[2,2048,256]{2,1,0:T(8,128)(2,1)S(1)}, bf16[2,2048,256]{2,1,0:T(8,128)(2,1)}, u32[]{:S(2)}) copy-start(bf16[2,2048,256]{2,1,0:T(8,128)(2,1)} %param.21) | copy-start | bytes 6291460
  45.3 1.7 %copy-start.5 = (bf16[2,2048,256]{2,1,0:T(8,128)(2,1)S(1)}, bf16[2,2048,256]{2,1,0:T(8,128)(2,1)}, u32[]{:S(2)}) copy-start(bf16[2,2048,256]{2,1,0:T(8,128)(2,1)} %param.22) | copy-start | bytes 6291460
  45.3 13.2 %collective-permute-start.3 = (bf16[128,2176]{1,0:T(8,128)(2,1)S(1)}, bf16[128,2176]{1,0:T(8,128)(2,1)S(1)}, u32[]{:S(2)}, u32[]{:S(2)}) collective-permute-start(bf16[128,2176]{1,0:T(8,128)(2,1)S(1)} %bitcast.87), channel_id=1, source_target_pairs={{0,2},{1,3},{2,0},{3,1},{4,6},{5,7},{6,4},{7,5},{8,10},{9,11},{10,... | collective-permute-start | bytes 1671176 | tf_op jit(solution)/shard_map/ppermute | solution.py:17
  46.1 2.0 %collective-permute-start.1 = (bf16[128,2176]{1,0:T(8,128)(2,1)S(1)}, bf16[128,2176]{1,0:T(8,128)(2,1)S(1)}, u32[]{:S(2)}, u32[]{:S(2)}) collective-permute-start(bf16[128,2176]{1,0:T(8,128)(2,1)S(1)} %bitcast.88), channel_id=1, source_target_pairs={{0,1},{1,0},{2,3},{3,2},{4,5},{5,4},{6,7},{7,6},{8,9},{9,8},{10,11... | collective-permute-start | bytes 1671176 | tf_op jit(solution)/shard_map/ppermute | solution.py:17
  58.4 2.0 %collective-permute-start.4 = (bf16[128,2176]{1,0:T(8,128)(2,1)S(1)}, bf16[128,2176]{1,0:T(8,128)(2,1)S(1)}, u32[]{:S(2)}, u32[]{:S(2)}) collective-permute-start(bf16[128,2176]{1,0:T(8,128)(2,1)S(1)} %collective-permute-done.3), channel_id=1, source_target_pairs={{0,1},{1,0},{2,3},{3,2},{4,5},{5,4},{6,7},{7,6},{8,9},{9,8},{10,11... | collective-permute-start | bytes 1671176 | tf_op jit(solution)/shard_map/ppermute | solution.py:17
  58.6 8.3 %collective-permute-start.2 = (bf16[128,2048]{1,0:T(8,128)(2,1)S(1)}, bf16[128,2048]{1,0:T(8,128)(2,1)S(1)}, u32[]{:S(2)}, u32[]{:S(2)}) collective-permute-start(bf16[128,2048]{1,0:T(8,128)(2,1)S(1)} %convolution_convert_fusion.2), channel_id=1, source_target_pairs={{0,1},{1,0},{2,3},{3,2},{4,5},{5,4},{6,7},{7,6},{8,9},{9,8},{10,11... | collective-permute-start | bytes 1572872 | tf_op jit(solution)/shard_map/ppermute | solution.py:17
  62.4 2.0 %collective-permute-start.5 = (bf16[128,2048]{1,0:T(8,128)(2,1)S(1)}, bf16[128,2048]{1,0:T(8,128)(2,1)S(1)}, u32[]{:S(2)}, u32[]{:S(2)}) collective-permute-start(bf16[128,2048]{1,0:T(8,128)(2,1)S(1)} %convolution_convert_fusion.1), channel_id=1, source_target_pairs={{0,1},{1,0},{2,3},{3,2},{4,5},{5,4},{6,7},{7,6},{8,9},{9,8},{10,11... | collective-permute-start | bytes 1572872 | tf_op jit(solution)/shard_map/ppermute | solution.py:17
  64.8 14.0 %collective-permute-start.6 = (bf16[128,2048]{1,0:T(8,128)(2,1)S(1)}, bf16[128,2048]{1,0:T(8,128)(2,1)S(1)}, u32[]{:S(2)}, u32[]{:S(2)}) collective-permute-start(bf16[128,2048]{1,0:T(8,128)(2,1)S(1)} %add_convert_fusion.1), channel_id=1, source_target_pairs={{0,2},{1,3},{2,0},{3,1},{4,6},{5,7},{6,4},{7,5},{8,10},{9,11},{10,... | collective-permute-start | bytes 1572872 | tf_op jit(solution)/shard_map/ppermute | solution.py:17
where the time goes:
time: 97.7 us; the launch traced here: 97.2 us
  blocking collectives  35.7 us (37%)
  waiting for transfers between devices  28.6 us (29%)
  matrix products  11.4 us (12%)
  starting transfers between devices  11.3 us (12%)
  other arithmetic  7.07 us (7%)
  local copies, waits for them, and re-layouts  2.75 us (3%)
    ppermute x6, waiting for transfers between devices, flipped(): lax.ppermute(block, axis, [(i, i ^ bit) for i in range(lax.axis_size(axis...  22.7 us
    all_to_all x1, blocking collectives, route_by_group(): lax.all_to_all(outgoing, 'sp', split_axis=0, concat_axis=0, tiled=True)  18.7 us
    all_to_all x1, blocking collectives, route_by_group(): lax.all_to_all(summed, 'sp', split_axis=0, concat_axis=0, tiled=True)  17 us
    all_to_all x1, waiting for transfers between devices, project(): lax.all_to_all(mixed, 'tp', split_axis=0, concat_axis=1, tiled=True)  5.94 us
    ppermute x1, starting transfers between devices, shifted(): return lax.ppermute(block, axis, route)  4.96 us
    all_to_all x1, starting transfers between devices, project(): lax.all_to_all(mixed, 'tp', split_axis=0, concat_axis=1, tiled=True)  3.41 us
    dot_general x1, matrix products, project(): jnp.dot(token_rows, out_proj, preferred_element_type=jnp.float32)  3.01 us
    ppermute x6, starting transfers between devices, flipped(): lax.ppermute(block, axis, [(i, i ^ bit) for i in range(lax.axis_size(axis...  2.97 us
  transfers between devices with their start and end apart: 8, of which 6 were waited for; matrix products, arithmetic and copies ran while one was open for 13% of the time, Pallas kernels for 0%

commit v1 on v0

--- a/solution.py
+++ b/solution.py
@@ -5,6 +5,18 @@
 
 GROUPS = 4
 LANES = 128
+
+
+def draw_the_face(block_in, row_dim, u):
+    lower = block_in.shape
+    z1 = block_in.reshape(*lower[:row_dim], u, lower[row_dim] // u, *lower[row_dim + 1 :])
+    return jnp.moveaxis(z1, row_dim, 0)
+
+
+def lift_points_by_axis(q_in, d0):
+    q_in = jnp.moveaxis(q_in, 0, d0)
+    shaped = q_in.shape
+    return q_in.reshape(*shaped[:d0], shaped[d0] * shaped[d0 + 1], *shaped[d0 + 2 :])
 
 
 def shifted(block, axis, distance):
@@ -62,7 +74,21 @@
     rows = jnp.concatenate([normed, labels], axis=1)
     outgoing = jnp.dot(select, rows, preferred_element_type=jnp.float32).astype(jnp.bfloat16)
     outgoing = outgoing.reshape(seq_ranks, capacity, width + LANES)
-    arrived = lax.all_to_all(outgoing, "sp", split_axis=0, concat_axis=0, tiled=True)
+    z_new = jax.lax.axis_size("sp")
+    current_block = jax.lax.axis_index("sp")
+    ready, moved = (z_new, current_block)
+    k_now = draw_the_face(outgoing, 0, ready)
+    by_place = [k_now[moved]]
+    for j0 in tuple(range(1, ready)):
+        aux = k_now[(moved + j0) % ready]
+        by_place.append(
+            jax.lax.ppermute(
+                aux, axis_name="sp", perm=[(i0, (i0 + j0) % ready) for i0 in range(ready)]
+            )
+        )
+    r2 = jnp.stack(by_place)
+    k_now = r2[(moved - jnp.arange(ready)) % ready]
+    arrived = lift_points_by_axis(k_now, 0)
     blocks = {0: arrived.reshape(block_rows, width + LANES)}
     bits = [1 << b for b in range(shards.bit_length() - 1)]
     for bit in reversed(bits):

time: 97.7 us -> 99.3 us (1.016)
  blocking collectives: 35.7 us -> 17.6 us
  waiting for transfers between devices: 28.6 us -> 36.9 us
  starting transfers between devices: 11.3 us -> 15.8 us
  matrix products: 11.4 us -> 14.1 us
  local copies, waits for them, and re-layouts: 2.75 us -> 5.26 us
  other arithmetic: 7.07 us -> 8.78 us
    all_to_all x1 -> x0, blocking collectives: 18.7 us -> none  [route_by_group(): lax.all_to_all(outgoing, 'sp', split_axis=0, concat_axis=0, tiled=True)]
    ppermute x0 -> x3, waiting for transfers between devices: none -> 10.4 us  [route_by_group(): jax.lax.ppermute(aux, axis_name='sp', perm=[(i0, (i0 + j0) % ready) for i...]
    ppermute x0 -> x3, starting transfers between devices: none -> 4.67 us  [route_by_group(): jax.lax.ppermute(aux, axis_name='sp', perm=[(i0, (i0 + j0) % ready) for i...]
    dot_general x8, matrix products: 2.56 us -> 5.22 us  [route_by_group(): gate = jnp.dot(features, w_gate[expert], preferred_element_type=jnp.float32)]
    gather x0 -> x1, local copies, waits for them, and re-layouts: none -> 2.45 us  [route_by_group(): k_now = r2[(moved - jnp.arange(ready)) % ready]]
    ppermute x6, waiting for transfers between devices: 22.7 us -> 20.5 us  [flipped(): lax.ppermute(block, axis, [(i, i ^ bit) for i in range(lax.axis_size(axis...]
  transfers between devices with their start and end apart: 8 -> 11, of which waited for: 6 -> 7; matrix products, arithmetic and copies ran while one was open for 13% -> 16% of each run, Pallas kernels for 0% -> 0%
where the time goes in v1:
time: 99.3 us; the launch traced here: 98.8 us
  waiting for transfers between devices  36.9 us (37%)
  blocking collectives  17.6 us (18%)
  starting transfers between devices  15.8 us (16%)
  matrix products  14.1 us (14%)
  other arithmetic  8.78 us (9%)
  local copies, waits for them, and re-layouts  5.26 us (5%)
    ppermute x6, waiting for transfers between devices, flipped(): lax.ppermute(block, axis, [(i, i ^ bit) for i in range(lax.axis_size(axis...  20.5 us
    all_to_all x1, blocking collectives, route_by_group(): lax.all_to_all(summed, 'sp', split_axis=0, concat_axis=0, tiled=True)  17.6 us
    ppermute x3, waiting for transfers between devices, route_by_group(): jax.lax.ppermute(aux, axis_name='sp', perm=[(i0, (i0 + j0) % ready) for i...  10.4 us
    all_to_all x1, waiting for transfers between devices, project(): lax.all_to_all(mixed, 'tp', split_axis=0, concat_axis=1, tiled=True)  5.94 us
    dot_general x8, matrix products, route_by_group(): gate = jnp.dot(features, w_gate[expert], preferred_element_type=jnp.float32)  5.22 us
    ppermute x1, starting transfers between devices, shifted(): return lax.ppermute(block, axis, route)  4.95 us
    ppermute x3, starting transfers between devices, route_by_group(): jax.lax.ppermute(aux, axis_name='sp', perm=[(i0, (i0 + j0) % ready) for i...  4.67 us
    all_to_all x1, starting transfers between devices, project(): lax.all_to_all(mixed, 'tp', split_axis=0, concat_axis=1, tiled=True)  3.41 us
  transfers between devices with their start and end apart: 11, of which 7 were waited for; matrix products, arithmetic and copies ran while one was open for 16% of the time, Pallas kernels for 0%

profile of v1, /device:TPU:0, one launch (start us, length us, event | category | flops | bytes accessed | tf_op | source)
XLA Modules:
  0.0 98.8 jit_solution(16989813809686866853)
XLA Ops:
  0.0 0.9 slice.127
  0.9 0.7 slice.128
  1.6 5.0 %collective-permute-start = (bf16[2,512]{1,0:T(2,128)(2,1)S(1)}, bf16[2,512]{1,0:T(2,128)(2,1)S(1)}, u32[]{:S(2)}, u32[]{:S(2)}) collective-permute-start(bf16[2,512]{1,0:T(2,128)(2,1)S(1)} %pad_maximum_fusion.1), channel_id=1, source_target_pairs={{0,4},{4,8},{8,12},{1,5},{5,9},{9,13},{2,6},{6,10},{10,14},{3,7},{... | collective-permute-start | bytes 6152 | tf_op jit(solution)/shard_map/ppermute | solution.py:25
  6.5 0.7 fusion.113
  7.2 0.7 and_select_fusion.3
  7.9 0.7 and_select_fusion.1
  8.6 1.1 %convert_multiply_fusion = f32[512,256]{1,0:T(8,128)S(1)} fusion(bf16[512,256]{1,0:T(8,128)(2,1)} %param.12, bf16[512,256]{1,0:T(8,128)(2,1)} %param.13), kind=kLoop, calls=%fused_computation.80 | loop fusion | flops 393216 | bytes 1048576 | tf_op jit(solution)/shard_map/mul | solution.py:41
  9.7 0.7 fusion.108
  10.6 0.9 fusion.121
  11.6 1.9 %fusion.62 = bf16[512,256]{1,0:T(8,128)(2,1)} fusion(f32[2,256]{1,0:T(2,128)S(1)} %convert_multiply_fusion.1, f32[512,256]{1,0:T(8,128)S(1)} %convert_multiply_fusion, bf16[512,256]{1,0:T(8,128)(2,1)} %param.14, f32[256]{0:T(256)S(1)} %bitcast.112, f32[256]{0:T(256)S(1)} %bitcast.111, f32[256]{0:T(256)S(1)} %bitcast.110), kind=kLoop, calls=%fused_computation.77 | loop fusion | flops 1310720 | bytes 1053696 | tf_op jit(solution)/shard_map/convert_element_type | solution.py:46
  13.5 3.4 %all-to-all-start = ((bf16[4,128,256]{2,1,0:T(8,128)(2,1)}), bf16[4,128,256]{2,1,0:T(8,128)(2,1)S(1)}, u32[]{:S(2)}, u32[]{:S(2)}) async-start(bf16[4,128,256]{2,1,0:T(8,128)(2,1)} %bitcast.3), calls=%async_computation | async-start | bytes 524288 | tf_op jit(solution)/shard_map/all_to_all | solution.py:50
  16.9 5.9 %all-to-all-done = bf16[4,128,256]{2,1,0:T(8,128)(2,1)S(1)} async-done(((bf16[4,128,256]{2,1,0:T(8,128)(2,1)}), bf16[4,128,256]{2,1,0:T(8,128)(2,1)S(1)}, u32[]{:S(2)}, u32[]{:S(2)}) %all-to-all-start) | async-done | bytes 262176 | tf_op jit(solution)/shard_map/all_to_all | solution.py:50
  23.1 3.1 %multiply_reduce_fusion = (f32[128]{0:T(128)S(1)}, f32[128,2048]{1,0:T(8,128)S(1)}) fusion(bf16[128,1024]{0,1:T(8,128)(2,1)S(1)} %bitcast.97, bf16[1024,2048]{1,0:T(8,128)(2,1)} %param.16, bf16[128,2048]{1,0:T(8,128)(2,1)} %param.17), kind=kOutput, calls=%fused_computation.48 | convolution fusion | flops 537919360 | bytes 6029824 | tf_op jit(solution)/shard_map/dot_general | solution.py:51
  26.7 1.5 %collective-permute-start.3 = (bf16[1,32,2176]{2,1,0:T(8,128)(2,1)S(1)}, bf16[1,32,2176]{2,1,0:T(8,128)(2,1)S(1)}, u32[]{:S(2)}, u32[]{:S(2)}) collective-permute-start(bf16[1,32,2176]{2,1,0:T(8,128)(2,1)S(1)} %get-tuple-element.14), channel_id=1, source_target_pairs={{0,12},{4,0},{8,4},{12,8},{1,13},{5,1},{9,5},{13,9},{2,14},{6,2},{... | collective-permute-start | bytes 417800 | tf_op jit(solution)/shard_map/ppermute | solution.py:85
  28.2 1.6 %collective-permute-start.2 = (bf16[1,32,2176]{2,1,0:T(8,128)(2,1)S(1)}, bf16[1,32,2176]{2,1,0:T(8,128)(2,1)S(1)}, u32[]{:S(2)}, u32[]{:S(2)}) collective-permute-start(bf16[1,32,2176]{2,1,0:T(8,128)(2,1)S(1)} %get-tuple-element.15), channel_id=1, source_target_pairs={{0,8},{4,12},{8,0},{12,4},{1,9},{5,13},{9,1},{13,5},{2,10},{6,14},... | collective-permute-start | bytes 417800 | tf_op jit(solution)/shard_map/ppermute | solution.py:85
  29.8 1.6 %collective-permute-start.1 = (bf16[1,32,2176]{2,1,0:T(8,128)(2,1)S(1)}, bf16[1,32,2176]{2,1,0:T(8,128)(2,1)S(1)}, u32[]{:S(2)}, u32[]{:S(2)}) collective-permute-start(bf16[1,32,2176]{2,1,0:T(8,128)(2,1)S(1)} %get-tuple-element.16), channel_id=1, source_target_pairs={{0,4},{4,8},{8,12},{12,0},{1,5},{5,9},{9,13},{13,1},{2,6},{6,10},{... | collective-permute-start | bytes 417800 | tf_op jit(solution)/shard_map/ppermute | solution.py:85
  31.4 0.9 collective-permute-done.3
  32.3 9.6 %collective-permute-done.2 = bf16[1,32,2176]{2,1,0:T(8,128)(2,1)S(1)} collective-permute-done((bf16[1,32,2176]{2,1,0:T(8,128)(2,1)S(1)}, bf16[1,32,2176]{2,1,0:T(8,128)(2,1)S(1)}, u32[]{:S(2)}, u32[]{:S(2)}) %collective-permute-start.2) | collective-permute-done | bytes 139296 | tf_op jit(solution)/shard_map/ppermute | solution.py:85
  41.9 0.9 maximum_bitcast_fusion
  42.8 2.5 %gather_fusion = bf16[4,32,2176]{2,1,0:T(8,128)(2,1)} fusion(bf16[4,32,2176]{2,1,0:T(8,128)(2,1)} %maximum_bitcast_fusion, s32[1024]{0:T(1024)S(1)} %pad_clamp_fusion), kind=kCustom, calls=%fused_computation | custom fusion | bytes 1114128 | tf_op jit(solution)/shard_map/gather | solution.py:90
  45.2 0.8 slice_convert_fusion.3
  46.1 0.8 collective-permute-start.6
  46.8 1.7 %fusion.19 = f32[128,256]{1,0:T(8,128)S(1)} fusion(bf16[2,2048,256]{2,1,0:T(8,128)(2,1)} %param.21, bf16[128,2176]{1,0:T(8,128)(2,1)} %bitcast.102), kind=kOutput, calls=%fused_computation.28 | convolution fusion | flops 134217728 | bytes 1703936 | tf_op jit(solution)/shard_map/dot_general | solution.py:103
  48.7 1.7 %fusion.34 = f32[128,256]{1,0:T(8,128)S(1)} fusion(bf16[2,2048,256]{2,1,0:T(8,128)(2,1)} %param.21, bf16[128,2176]{1,0:T(8,128)(2,1)S(1)} %bitcast.103), kind=kOutput, calls=%fused_computation.43 | convolution fusion | flops 134217728 | bytes 1703936 | tf_op jit(solution)/shard_map/dot_general | solution.py:103
  50.4 0.3 fusion.4
  51.0 0.3 fusion.17
  51.6 0.3 multiply_convert_fusion.5
  51.9 0.3 multiply_convert_fusion.6
  52.3 0.4 convolution_convert_fusion.2
  52.7 6.8 %collective-permute-done.6 = bf16[128,2176]{1,0:T(8,128)(2,1)S(1)} collective-permute-done((bf16[128,2176]{1,0:T(8,128)(2,1)}, bf16[128,2176]{1,0:T(8,128)(2,1)S(1)}, u32[]{:S(2)}, u32[]{:S(2)}) %collective-permute-start.6) | collective-permute-done | bytes 557088 | tf_op jit(solution)/shard_map/ppermute | solution.py:29
  59.7 0.6 collective-permute-start.5
  60.6 0.3 multiply_convert_fusion.3
  60.9 0.6 collective-permute-done.7
  61.6 0.3 fusion.13
  62.0 0.3 fusion.28
  62.3 0.3 multiply_convert_fusion.1
  62.6 0.3 multiply_convert_fusion.2
  62.9 0.4 convolution_convert_fusion.1
  63.6 0.3 fusion.30
  63.9 0.3 multiply_convert_fusion.4
  64.2 1.1 %collective-permute-done.8 = bf16[128,2048]{1,0:T(8,128)(2,1)S(1)} collective-permute-done((bf16[128,2048]{1,0:T(8,128)(2,1)S(1)}, bf16[128,2048]{1,0:T(8,128)(2,1)S(1)}, u32[]{:S(2)}, u32[]{:S(2)}) %collective-permute-start.8) | collective-permute-done | bytes 524320 | tf_op jit(solution)/shard_map/ppermute | solution.py:29
  65.4 0.4 add_convert_fusion.1
  65.8 1.2 %collective-permute-start.9 = (bf16[128,2048]{1,0:T(8,128)(2,1)S(1)}, bf16[128,2048]{1,0:T(8,128)(2,1)S(1)}, u32[]{:S(2)}, u32[]{:S(2)}) collective-permute-start(bf16[128,2048]{1,0:T(8,128)(2,1)S(1)} %add_convert_fusion.1), channel_id=1, source_target_pairs={{0,2},{1,3},{2,0},{3,1},{4,6},{5,7},{6,4},{7,5},{8,10},{9,11},{10,... | collective-permute-start | bytes 1572872 | tf_op jit(solution)/shard_map/ppermute | solution.py:29
  67.0 0.3 fusion.3
  67.3 0.4 fusion.81
  67.8 12.1 %collective-permute-done.9 = bf16[128,2048]{1,0:T(8,128)(2,1)S(1)} collective-permute-done((bf16[128,2048]{1,0:T(8,128)(2,1)S(1)}, bf16[128,2048]{1,0:T(8,128)(2,1)S(1)}, u32[]{:S(2)}, u32[]{:S(2)}) %collective-permute-start.9) | collective-permute-done | bytes 524320 | tf_op jit(solution)/shard_map/ppermute | solution.py:29
  80.0 17.6 %all_to_all.24 = bf16[4,32,2048]{2,1,0:T(8,128)(2,1)S(1)} all-to-all(bf16[4,32,2048]{2,1,0:T(8,128)(2,1)S(1)} %bitcast.95), channel_id=1, replica_groups=mesh['grp'=2,'sp'=4,'tp'=4] {'sp'}, dimensions={0} | all-to-all | bytes 1048576 | tf_op jit(solution)/shard_map/all_to_all | solution.py:115
  97.7 1.1 %fusion = bf16[128,2048]{1,0:T(8,128)(2,1)} fusion(f32[128,2048]{1,0:T(8,128)S(1)} %get-tuple-element.23, bf16[128,2048]{1,0:T(8,128)(2,1)S(1)} %bitcast.96, s32[128]{0:T(128)S(1)} %multiply_add_fusion), kind=kOutput, calls=%fused_computation.4 | convolution fusion | flops 67649536 | bytes 2097664 | tf_op jit(solution)/shard_map/dot_general | solution.py:116
  (43 shorter events, 2.9 us)
Async XLA Ops:
  0.0 52.2 %copy-start = (bf16[2,256,2048]{2,1,0:T(8,128)(2,1)S(1)}, bf16[2,256,2048]{2,1,0:T(8,128)(2,1)}, u32[]{:S(2)}) copy-start(bf16[2,256,2048]{2,1,0:T(8,128)(2,1)} %param.23) | copy-start | bytes 6291460
  0.0 16.9 %copy-start.3 = (s32[128,2]{0,1:T(2,128)S(1)}, s32[128,2]{0,1:T(2,128)}, u32[]{:S(2)}) copy-start(s32[128,2]{0,1:T(2,128)} %param.19) | copy-start | bytes 3076
  1.6 10.0 %collective-permute-start = (bf16[2,512]{1,0:T(2,128)(2,1)S(1)}, bf16[2,512]{1,0:T(2,128)(2,1)S(1)}, u32[]{:S(2)}, u32[]{:S(2)}) collective-permute-start(bf16[2,512]{1,0:T(2,128)(2,1)S(1)} %pad_maximum_fusion.1), channel_id=1, source_target_pairs={{0,4},{4,8},{8,12},{1,5},{5,9},{9,13},{2,6},{6,10},{10,14},{3,7},{... | collective-permute-start | bytes 6152 | tf_op jit(solution)/shard_map/ppermute | solution.py:25
  13.5 9.4 %all-to-all-start = ((bf16[4,128,256]{2,1,0:T(8,128)(2,1)}), bf16[4,128,256]{2,1,0:T(8,128)(2,1)S(1)}, u32[]{:S(2)}, u32[]{:S(2)}) async-start(bf16[4,128,256]{2,1,0:T(8,128)(2,1)} %bitcast.3), calls=%async_computation | async-start | bytes 524288 | tf_op jit(solution)/shard_map/all_to_all | solution.py:50
  23.0 3.2 %copy-start.2 = (f32[2048]{0:T(1024)S(1)}, f32[2048]{0:T(1024)}, u32[]{:S(2)}) copy-start(f32[2048]{0:T(1024)} %param.18) | copy-start | bytes 24580
  26.7 5.6 %collective-permute-start.3 = (bf16[1,32,2176]{2,1,0:T(8,128)(2,1)S(1)}, bf16[1,32,2176]{2,1,0:T(8,128)(2,1)S(1)}, u32[]{:S(2)}, u32[]{:S(2)}) collective-permute-start(bf16[1,32,2176]{2,1,0:T(8,128)(2,1)S(1)} %get-tuple-element.14), channel_id=1, source_target_pairs={{0,12},{4,0},{8,4},{12,8},{1,13},{5,1},{9,5},{13,9},{2,14},{6,2},{... | collective-permute-start | bytes 417800 | tf_op jit(solution)/shard_map/ppermute | solution.py:85
  28.2 13.7 %collective-permute-start.2 = (bf16[1,32,2176]{2,1,0:T(8,128)(2,1)S(1)}, bf16[1,32,2176]{2,1,0:T(8,128)(2,1)S(1)}, u32[]{:S(2)}, u32[]{:S(2)}) collective-permute-start(bf16[1,32,2176]{2,1,0:T(8,128)(2,1)S(1)} %get-tuple-element.15), channel_id=1, source_target_pairs={{0,8},{4,12},{8,0},{12,4},{1,9},{5,13},{9,1},{13,5},{2,10},{6,14},... | collective-permute-start | bytes 417800 | tf_op jit(solution)/shard_map/ppermute | solution.py:85
  29.8 12.0 %collective-permute-start.1 = (bf16[1,32,2176]{2,1,0:T(8,128)(2,1)S(1)}, bf16[1,32,2176]{2,1,0:T(8,128)(2,1)S(1)}, u32[]{:S(2)}, u32[]{:S(2)}) collective-permute-start(bf16[1,32,2176]{2,1,0:T(8,128)(2,1)S(1)} %get-tuple-element.16), channel_id=1, source_target_pairs={{0,4},{4,8},{8,12},{12,0},{1,5},{5,9},{9,13},{13,1},{2,6},{6,10},{... | collective-permute-start | bytes 417800 | tf_op jit(solution)/shard_map/ppermute | solution.py:85
  45.2 3.5 %copy-start.1 = (bf16[4,32,2176]{2,1,0:T(8,128)(2,1)S(1)}, bf16[4,32,2176]{2,1,0:T(8,128)(2,1)}, u32[]{:S(2)}) copy-start(bf16[4,32,2176]{2,1,0:T(8,128)(2,1)} %gather_fusion) | copy-start | bytes 1671172
  46.1 4.4 %copy-start.5 = (bf16[2,2048,256]{2,1,0:T(8,128)(2,1)S(1)}, bf16[2,2048,256]{2,1,0:T(8,128)(2,1)}, u32[]{:S(2)}) copy-start(bf16[2,2048,256]{2,1,0:T(8,128)(2,1)} %param.22) | copy-start | bytes 6291460
  46.1 13.4 %collective-permute-start.6 = (bf16[128,2176]{1,0:T(8,128)(2,1)}, bf16[128,2176]{1,0:T(8,128)(2,1)S(1)}, u32[]{:S(2)}, u32[]{:S(2)}) collective-permute-start(bf16[128,2176]{1,0:T(8,128)(2,1)} %bitcast.100), channel_id=1, source_target_pairs={{0,2},{1,3},{2,0},{3,1},{4,6},{5,7},{6,4},{7,5},{8,10},{9,11},{10,... | collective-permute-start | bytes 1671176 | tf_op jit(solution)/shard_map/ppermute | solution.py:29
  46.8 3.9 %collective-permute-start.4 = (bf16[128,2176]{1,0:T(8,128)(2,1)}, bf16[128,2176]{1,0:T(8,128)(2,1)S(1)}, u32[]{:S(2)}, u32[]{:S(2)}) collective-permute-start(bf16[128,2176]{1,0:T(8,128)(2,1)} %bitcast.101), channel_id=1, source_target_pairs={{0,1},{1,0},{2,3},{3,2},{4,5},{5,4},{6,7},{7,6},{8,9},{9,8},{10,11... | collective-permute-start | bytes 1671176 | tf_op jit(solution)/shard_map/ppermute | solution.py:29
  48.7 2.3 %copy-start.4 = (bf16[2,2048,256]{2,1,0:T(8,128)(2,1)S(1)}, bf16[2,2048,256]{2,1,0:T(8,128)(2,1)}, u32[]{:S(2)}) copy-start(bf16[2,2048,256]{2,1,0:T(8,128)(2,1)} %param.21) | copy-start | bytes 6291460
  59.5 2.0 %collective-permute-start.7 = (bf16[128,2176]{1,0:T(8,128)(2,1)S(1)}, bf16[128,2176]{1,0:T(8,128)(2,1)S(1)}, u32[]{:S(2)}, u32[]{:S(2)}) collective-permute-start(bf16[128,2176]{1,0:T(8,128)(2,1)S(1)} %collective-permute-done.6), channel_id=1, source_target_pairs={{0,1},{1,0},{2,3},{3,2},{4,5},{5,4},{6,7},{7,6},{8,9},{9,8},{10,11... | collective-permute-start | bytes 1671176 | tf_op jit(solution)/shard_map/ppermute | solution.py:29
  59.7 8.1 %collective-permute-start.5 = (bf16[128,2048]{1,0:T(8,128)(2,1)S(1)}, bf16[128,2048]{1,0:T(8,128)(2,1)S(1)}, u32[]{:S(2)}, u32[]{:S(2)}) collective-permute-start(bf16[128,2048]{1,0:T(8,128)(2,1)S(1)} %convolution_convert_fusion.2), channel_id=1, source_target_pairs={{0,1},{1,0},{2,3},{3,2},{4,5},{5,4},{6,7},{7,6},{8,9},{9,8},{10,11... | collective-permute-start | bytes 1572872 | tf_op jit(solution)/shard_map/ppermute | solution.py:29
  63.4 2.0 %collective-permute-start.8 = (bf16[128,2048]{1,0:T(8,128)(2,1)S(1)}, bf16[128,2048]{1,0:T(8,128)(2,1)S(1)}, u32[]{:S(2)}, u32[]{:S(2)}) collective-permute-start(bf16[128,2048]{1,0:T(8,128)(2,1)S(1)} %convolution_convert_fusion.1), channel_id=1, source_target_pairs={{0,1},{1,0},{2,3},{3,2},{4,5},{5,4},{6,7},{7,6},{8,9},{9,8},{10,11... | collective-permute-start | bytes 1572872 | tf_op jit(solution)/shard_map/ppermute | solution.py:29
  65.8 14.0 %collective-permute-start.9 = (bf16[128,2048]{1,0:T(8,128)(2,1)S(1)}, bf16[128,2048]{1,0:T(8,128)(2,1)S(1)}, u32[]{:S(2)}, u32[]{:S(2)}) collective-permute-start(bf16[128,2048]{1,0:T(8,128)(2,1)S(1)} %add_convert_fusion.1), channel_id=1, source_target_pairs={{0,2},{1,3},{2,0},{3,1},{4,6},{5,7},{6,4},{7,5},{8,10},{9,11},{10,... | collective-permute-start | bytes 1572872 | tf_op jit(solution)/shard_map/ppermute | solution.py:29
